TPU v7x, 32 devices: a whole 2x2x4 slice. The times are simulated.
32 devices in a mesh: sp: 8 (over z, y), tp: 4 (over x, core).
Axes of the slice: x: 2, y: 2, z: 4, core: 2. Of those that a mesh axis runs over, the one named last changes fastest.
Arguments:
- target: bfloat16 [1024, 2048], P('sp'), may hold values from -160 to 160
- source: bfloat16 [2048, 2048], P(('sp', 'tp')), may hold values from -160 to 160
- query_gain: float32 [2048], replicated, may hold values from 0.1 to 1.9
- source_gain: float32 [2048], replicated, may hold values from 0.1 to 1.9
- query_weight: bfloat16 [2048, 2048], P(None, 'tp'), may hold values from -4 to 4
- key_weight: bfloat16 [2048, 512], replicated, may hold values from -4 to 4
- value_weight: bfloat16 [2048, 512], replicated, may hold values from -1 to 1
- out_weight: bfloat16 [2048, 2048], P('tp'), may hold values from -0.125 to 0.125
- mixer_gain: float32 [2048], replicated, may hold values from 0.1 to 1.9
- gate_weight: bfloat16 [2048, 3072], P(None, 'tp'), may hold values from -0.125 to 0.125
- up_weight: bfloat16 [2048, 3072], P(None, 'tp'), may hold values from -0.125 to 0.125
- gate_taps: bfloat16 [3, 3072], P(None, 'tp'), may hold values from -3.5 to 3.5
- up_taps: bfloat16 [3, 3072], P(None, 'tp'), may hold values from -3.5 to 3.5
- down_weight: bfloat16 [3072, 2048], P('tp'), may hold values from -0.109375 to 0.109375
- final_gain: float32 [2048], replicated, may hold values from 0.1 to 1.9
Outputs:
- layer_out: bfloat16 [1024, 2048], P(('sp', 'tp'))
All inputs are finite; a program needn't handle non-finite values.
Results may differ from a plain program's by a relative error of at most 0.012.
Values may be sent and summed in bfloat16 or wider, within the bound.
A program may use at most 64 MiB of HBM per device.

v0:
```python
import math

import jax
import jax.numpy as jnp
from jax import lax
from jax.sharding import PartitionSpec as P

D = 2048
HEADS = 8
HEAD = 256
KV_HEADS = 2
CONV = 3
TGT_DEV = 128


EPS = 1e-06


def passed_along(shard, axis, by):
    peers = lax.axis_size(axis)
    pairs = [(i, i + by) for i in range(peers) if 0 <= i + by < peers]
    return lax.ppermute(shard, axis, pairs)


def normalize(values, gain):
    widened = values.astype(jnp.float32)
    scaled = widened * lax.rsqrt(jnp.mean(widened * widened, axis=-1, keepdims=True) + EPS)
    return (scaled * gain).astype(jnp.bfloat16)


def shards(
    target,
    source,
    query_gain,
    source_gain,
    query_weight,
    key_weight,
    value_weight,
    out_weight,
    mixer_gain,
    gate_weight,
    up_weight,
    gate_taps,
    up_taps,
    down_weight,
    final_gain,
):
    tp_count = lax.axis_size("tp")
    heads_here = HEADS // tp_count
    group_size = HEADS // KV_HEADS
    row_share = TGT_DEV // tp_count
    first_mine = lax.axis_index("tp") * row_share
    score_scale = HEAD ** (-0.5)
    normed = normalize(target, query_gain)
    own_query = jnp.dot(normed, query_weight, preferred_element_type=jnp.float32).astype(
        jnp.bfloat16
    )
    own_query = own_query.reshape(TGT_DEV, heads_here, HEAD).transpose(1, 0, 2)
    queries = lax.all_gather(own_query, "tp", axis=0, tiled=True)
    grouped = queries.reshape(KV_HEADS, group_size * TGT_DEV, HEAD)
    source_normed = normalize(source, source_gain)
    key_rows = jnp.dot(source_normed, key_weight, preferred_element_type=jnp.float32).astype(
        jnp.bfloat16
    )
    value_rows = jnp.dot(source_normed, value_weight, preferred_element_type=jnp.float32).astype(
        jnp.bfloat16
    )
    keys_all, values_all = (
        lax.all_gather(key_rows, "sp", axis=0, tiled=True),
        lax.all_gather(value_rows, "sp", axis=0, tiled=True),
    )
    total_keys = keys_all.shape[0]
    block_rows = math.gcd(total_keys, 512)
    block_count = total_keys // block_rows

    def absorb(block_index, state_now):
        running_max, running_sum, weighted = state_now
        first_row = block_index * block_rows
        key_heads = lax.dynamic_slice_in_dim(keys_all, first_row, block_rows, 0).reshape(
            block_rows, KV_HEADS, HEAD
        )
        value_heads = lax.dynamic_slice_in_dim(values_all, first_row, block_rows, 0).reshape(
            block_rows, KV_HEADS, HEAD
        )
        scores = (
            jnp.einsum("gqd,ngd->gqn", grouped, key_heads, preferred_element_type=jnp.float32)
            * score_scale
        )
        new_max = jnp.maximum(running_max, jnp.max(scores, axis=-1))
        shrink = jnp.exp(running_max - new_max)
        probabilities = jnp.exp(scores - new_max[..., None])
        running_sum = running_sum * shrink + jnp.sum(probabilities, axis=-1)
        weighted = weighted * shrink[..., None] + jnp.einsum(
            "gqn,ngd->gqd",
            probabilities.astype(jnp.bfloat16),
            value_heads,
            preferred_element_type=jnp.float32,
        )
        return (new_max, running_sum, weighted)

    start_state = (
        jnp.full((KV_HEADS, group_size * TGT_DEV), -1e30, jnp.float32),
        jnp.zeros((KV_HEADS, group_size * TGT_DEV), jnp.float32),
        jnp.zeros((KV_HEADS, group_size * TGT_DEV, HEAD), jnp.float32),
    )
    running_max, running_sum, weighted = lax.fori_loop(0, block_count, absorb, start_state)
    running_max = running_max.reshape(1, HEADS, TGT_DEV)
    running_sum = running_sum.reshape(1, HEADS, TGT_DEV)
    weighted = weighted.reshape(1, HEADS, TGT_DEV, HEAD)
    maxima, totals, partial_sums = (
        lax.all_to_all(running_max, "tp", split_axis=1, concat_axis=0, tiled=True),
        lax.all_to_all(running_sum, "tp", split_axis=1, concat_axis=0, tiled=True),
        lax.all_to_all(weighted, "tp", split_axis=1, concat_axis=0, tiled=True),
    )
    highest = jnp.max(maxima, axis=0)
    factor = jnp.exp(maxima - highest)
    denominator = jnp.sum(factor * totals, axis=0)
    merged = (jnp.sum(factor[..., None] * partial_sums, axis=0) / denominator[..., None]).astype(
        jnp.bfloat16
    )
    out_heads = out_weight.reshape(heads_here, HEAD, D)
    row_block = merged
    projected = lax.psum_scatter(
        jnp.einsum("hrd,hdc->rc", row_block, out_heads, preferred_element_type=jnp.float32),
        "tp",
        scatter_dimension=0,
        tiled=True,
    )
    target_rows = lax.dynamic_slice_in_dim(target, first_mine, row_share, 0)
    residual_rows = (target_rows.astype(jnp.float32) + projected).astype(jnp.bfloat16)
    arrived = lax.all_gather(normalize(residual_rows, mixer_gain), "tp", axis=0, tiled=True)
    gate_up = jnp.stack(
        [
            jnp.dot(arrived, gate_weight, preferred_element_type=jnp.float32).astype(jnp.bfloat16),
            jnp.dot(arrived, up_weight, preferred_element_type=jnp.float32).astype(jnp.bfloat16),
        ]
    )
    tail_rows = gate_up[:, TGT_DEV - (CONV - 1) :, :]
    earlier = passed_along(tail_rows, "sp", 1)
    padded = jnp.concatenate([earlier, gate_up], axis=1).astype(jnp.float32)
    conv_taps = jnp.stack([gate_taps, up_taps]).astype(jnp.float32)
    mixed = conv_taps[:, 0:1, :] * padded[:, 0:TGT_DEV, :]
    for index_tap in range(1, CONV):
        mixed = (
            mixed
            + conv_taps[:, index_tap : index_tap + 1, :]
            * padded[:, index_tap : index_tap + TGT_DEV, :]
        )
    hidden = (jax.nn.silu(mixed[0]) * mixed[1]).astype(jnp.bfloat16)
    row_block = hidden
    mixer = lax.psum_scatter(
        jnp.dot(row_block, down_weight, preferred_element_type=jnp.float32),
        "tp",
        scatter_dimension=0,
        tiled=True,
    )
    return normalize(residual_rows.astype(jnp.float32) + mixer, final_gain)


def solution(mesh):
    in_specs = (
        P("sp", None),
        P(("sp", "tp"), None),
        P(),
        P(),
        P(None, "tp"),
        P(),
        P(),
        P("tp", None),
        P(),
        P(None, "tp"),
        P(None, "tp"),
        P(None, "tp"),
        P(None, "tp"),
        P("tp", None),
        P(),
    )
    out_specs = P(("sp", "tp"), None)
    return jax.shard_map(shards, mesh=mesh, in_specs=in_specs, out_specs=out_specs, check_vma=False)
```

profile of v0, /device:TPU:0, one launch (start us, length us, event | category | flops | bytes accessed | tf_op | source)
XLA Modules:
  0.0 205.2 jit_solution(9786807580128010057)
XLA Ops:
  6.5 1.3 fusion.12
  7.8 2.3 %convolution_convert_fusion.4 = bf16[64,512]{1,0:T(8,128)(2,1)S(1)} fusion(bf16[2048,512]{1,0:T(8,128)(2,1)} %param.20, bf16[64,2048]{1,0:T(8,128)(2,1)} %param.16, f32[2048]{0:T(1024)} %param.18, f32[64]{0:T(128)S(1)} %add_rsqrt_fusion.2), kind=kOutput, calls=%fused_computation.14 | convolution fusion | flops 134774784 | bytes 2433280 | tf_op jit(solution)/shard_map/dot_general | solution.py:62
  10.2 33.0 %all_gather.13 = bf16[512,512]{1,0:T(8,128)(2,1)S(1)} all-gather(bf16[64,512]{1,0:T(8,128)(2,1)S(1)} %convolution_convert_fusion.4), channel_id=1, replica_groups=mesh['sp'=8,'tp'=4] {'sp'}, dimensions={0}, use_global_device_ids=true | all-gather | bytes 589824 | tf_op jit(solution)/shard_map/all_gather | solution.py:69
  43.4 0.5 convolution_convert_fusion.2
  43.9 7.2 %all_gather.12 = bf16[8,128,256]{2,1,0:T(8,128)(2,1)S(1)} all-gather(bf16[2,128,256]{2,1,0:T(8,128)(2,1)S(1)} %bitcast.67), channel_id=1, replica_groups=mesh['sp'=8,'tp'=4] {'tp'}, dimensions={0}, use_global_device_ids=true | all-gather | bytes 655360 | tf_op jit(solution)/shard_map/all_gather | solution.py:59
  51.1 1.8 multiply_reduce_fusion
  52.9 0.6 max.26
  53.6 2.0 fusion
  55.5 1.3 multiply_add_fusion
  56.8 3.2 %all-to-all-start.2 = ((f32[1,8,128]{2,0,1:T(1,128)}), f32[1,8,128]{2,0,1:T(1,128)S(1)}, u32[]{:S(2)}, u32[]{:S(2)}) async-start(f32[1,8,128]{2,0,1:T(1,128)} %multiply_add_fusion), calls=%async_computation.2 | async-start | bytes 8192 | tf_op jit(solution)/shard_map/all_to_all | solution.py:112
  60.1 2.1 %convolution_convert_fusion.3 = bf16[64,512]{1,0:T(8,128)(2,1)S(1)} fusion(bf16[2048,512]{1,0:T(8,128)(2,1)} %param.21, bf16[64,2048]{1,0:T(8,128)(2,1)S(1)} %copy-done.2, f32[2048]{0:T(1024)S(1)} %copy-done.4, f32[64]{0:T(128)S(1)} %add_rsqrt_fusion.2), kind=kOutput, calls=%fused_computation.13 | convolution fusion | flops 134774784 | bytes 2433280 | tf_op jit(solution)/shard_map/dot_general | solution.py:65
  62.2 33.2 %all_gather.14 = bf16[512,512]{1,0:T(8,128)(2,1)} all-gather(bf16[64,512]{1,0:T(8,128)(2,1)S(1)} %convolution_convert_fusion.3), channel_id=1, replica_groups=mesh['sp'=8,'tp'=4] {'sp'}, dimensions={0}, use_global_device_ids=true | all-gather | bytes 589824 | tf_op jit(solution)/shard_map/all_gather | solution.py:70
  95.4 3.4 %all-to-all-start = ((f32[1,8,128]{2,0,1:T(1,128)}), f32[1,8,128]{2,0,1:T(1,128)S(1)}, u32[]{:S(2)}, u32[]{:S(2)}) async-start(f32[1,8,128]{2,0,1:T(1,128)} %max.26), calls=%async_computation | async-start | bytes 8192 | tf_op jit(solution)/shard_map/all_to_all | solution.py:111
  98.8 3.3 %convolution_add_fusion = f32[2,512,256]{2,1,0:T(8,128)} fusion(f32[2,512,512]{1,2,0:T(8,128)} %get-tuple-element.39, f32[2,512]{1,0:T(2,128)S(1)} %get-tuple-element.37, bf16[64,2,8,256]{3,2,1,0:T(8,128)(2,1)} %bitcast.64, f32[2,512]{1,0:T(2,128)S(1)} %get-tuple-element.36), kind=kOutput, calls=%fused_computation.5 | convolution fusion | flops 270270464 | bytes 3678208 | tf_op jit(solution)/shard_map/while/body/eval_jaxpr/gqn,ngd->gqd/dot_general | solution.py:93
  102.1 0.5 all-to-all-done
  102.6 4.2 %all-to-all-start.1 = ((f32[1,8,128,256]{3,2,0,1:T(8,128)}), f32[1,8,128,256]{3,2,0,1:T(8,128)}, u32[]{:S(2)}, u32[]{:S(2)}) async-start(f32[1,8,128,256]{3,2,0,1:T(8,128)} %bitcast.62), calls=%async_computation.1 | async-start | bytes 2097152 | tf_op jit(solution)/shard_map/all_to_all | solution.py:113
  106.9 14.4 %all-to-all-done.1 = f32[1,8,128,256]{3,2,0,1:T(8,128)} async-done(((f32[1,8,128,256]{3,2,0,1:T(8,128)}), f32[1,8,128,256]{3,2,0,1:T(8,128)}, u32[]{:S(2)}, u32[]{:S(2)}) %all-to-all-start.1) | async-done | bytes 1048608 | tf_op jit(solution)/shard_map/all_to_all | solution.py:113
  121.3 1.4 multiply_reduce_fusion.1
  122.8 3.1 %convolution_bitcast_fusion = f32[128,2048]{1,0:T(8,128)} fusion(bf16[2,256,2048]{2,1,0:T(8,128)(2,1)} %bitcast.63, f32[2,128,256]{2,1,0:T(8,128)S(1)} %multiply_reduce_fusion.1, f32[2,128]{1,0:T(2,128)S(1)} %get-tuple-element.21), kind=kOutput, calls=%fused_computation | convolution fusion | flops 268566528 | bytes 3408896 | tf_op jit(solution)/shard_map/hrd,hdc->rc/dot_general | solution.py:124
  126.0 25.2 %reduce-scatter.3.cloned.1.call-done = f32[32,2048]{1,0:T(8,128)} async-done(((f32[128,2048]{1,0:T(8,128)}), f32[32,2048]{1,0:T(8,128)}) %reduce-scatter.3.cloned.1.call-update) | async-done | bytes 262160 | tf_op jit(solution)/shard_map/reduce_scatter | solution.py:123
  151.2 1.1 fusion.25
  152.5 6.6 %all_gather.15 = bf16[128,2048]{1,0:T(8,128)(2,1)S(1)} all-gather(bf16[32,2048]{1,0:T(8,128)(2,1)S(1)} %fusion.27), channel_id=1, replica_groups=mesh['sp'=8,'tp'=4] {'tp'}, dimensions={0}, use_global_device_ids=true | all-gather | bytes 655360 | tf_op jit(solution)/shard_map/all_gather | solution.py:131
  159.1 2.6 %fusion.2 = bf16[1,128,768]{2,1,0:T(8,128)(2,1)S(1)} fusion(bf16[128,2048]{1,0:T(8,128)(2,1)S(1)} %all_gather.15, bf16[2048,768]{1,0:T(8,128)(2,1)} %param.24), kind=kOutput, calls=%fused_computation.11 | convolution fusion | flops 402751488 | bytes 3866624 | tf_op jit(solution)/shard_map/dot_general | solution.py:134
  161.7 0.2 copy-done.1
  161.9 0.6 fusion.3
  162.5 3.4 %collective-permute-start = (bf16[2,2,768]{2,1,0:T(2,128)(2,1)S(1)}, bf16[2,2,768]{2,1,0:T(2,128)(2,1)S(1)}, u32[]{:S(2)}, u32[]{:S(2)}) collective-permute-start(bf16[2,2,768]{2,1,0:T(2,128)(2,1)S(1)} %pad_maximum_fusion.1), channel_id=1, source_target_pairs={{0,4},{4,8},{8,12},{12,16},{16,20},{20,24},{24,28},{1,5},{5,9},{9,... | collective-permute-start | bytes 18440 | tf_op jit(solution)/shard_map/ppermute | solution.py:22
  165.9 1.3 collective-permute-done
  167.3 0.2 fusion.10
  167.6 1.6 fusion.28
  169.2 26.3 %reduce-scatter.5.cloned.1.call-done = f32[32,2048]{1,0:T(8,128)} async-done(((f32[128,2048]{1,0:T(8,128)}), f32[32,2048]{1,0:T(8,128)}) %reduce-scatter.5.cloned.1.call-update) | async-done | bytes 262160 | tf_op jit(solution)/shard_map/reduce_scatter | solution.py:151
  195.5 1.1 multiply_reduce_fusion.2
  196.6 1.7 multiply_convert_fusion
  (42 shorter events, 0.7 us)
Async XLA Ops:
  6.5 161.0 %copy-start = (bf16[768,2048]{1,0:T(8,128)(2,1)S(1)}, bf16[768,2048]{1,0:T(8,128)(2,1)}, u32[]{:S(2)}) copy-start(bf16[768,2048]{1,0:T(8,128)(2,1)} %param.28) | copy-start | bytes 9437188
  6.5 36.7 %copy-start.3 = (bf16[128,2048]{1,0:T(8,128)(2,1)S(1)}, bf16[128,2048]{1,0:T(8,128)(2,1)}, u32[]{:S(2)}) copy-start(bf16[128,2048]{1,0:T(8,128)(2,1)} %param.15) | copy-start | bytes 1572868
  6.5 36.9 %copy-start.10 = (f32[2048]{0:T(1024)S(1)}, f32[2048]{0:T(1024)}, u32[]{:S(2)}) copy-start(f32[2048]{0:T(1024)} %param.17) | copy-start | bytes 24580
  6.5 36.9 %copy-start.9 = (bf16[2048,512]{1,0:T(8,128)(2,1)S(1)}, bf16[2048,512]{1,0:T(8,128)(2,1)}, u32[]{:S(2)}) copy-start(bf16[2048,512]{1,0:T(8,128)(2,1)} %param.19) | copy-start | bytes 6291460
  51.1 9.0 %copy-start.2 = (bf16[64,2048]{1,0:T(8,128)(2,1)S(1)}, bf16[64,2048]{1,0:T(8,128)(2,1)}, u32[]{:S(2)}) copy-start(bf16[64,2048]{1,0:T(8,128)(2,1)} %param.16) | copy-start | bytes 786436
  51.1 9.0 %copy-start.4 = (f32[2048]{0:T(1024)S(1)}, f32[2048]{0:T(1024)}, u32[]{:S(2)}) copy-start(f32[2048]{0:T(1024)} %param.18) | copy-start | bytes 24580
  56.8 38.6 %all-to-all-start.2 = ((f32[1,8,128]{2,0,1:T(1,128)}), f32[1,8,128]{2,0,1:T(1,128)S(1)}, u32[]{:S(2)}, u32[]{:S(2)}) async-start(f32[1,8,128]{2,0,1:T(1,128)} %multiply_add_fusion), calls=%async_computation.2 | async-start | bytes 8192 | tf_op jit(solution)/shard_map/all_to_all | solution.py:112
  95.4 7.2 %all-to-all-start = ((f32[1,8,128]{2,0,1:T(1,128)}), f32[1,8,128]{2,0,1:T(1,128)S(1)}, u32[]{:S(2)}, u32[]{:S(2)}) async-start(f32[1,8,128]{2,0,1:T(1,128)} %max.26), calls=%async_computation | async-start | bytes 8192 | tf_op jit(solution)/shard_map/all_to_all | solution.py:111
  102.6 18.7 %all-to-all-start.1 = ((f32[1,8,128,256]{3,2,0,1:T(8,128)}), f32[1,8,128,256]{3,2,0,1:T(8,128)}, u32[]{:S(2)}, u32[]{:S(2)}) async-start(f32[1,8,128,256]{3,2,0,1:T(8,128)} %bitcast.62), calls=%async_computation.1 | async-start | bytes 2097152 | tf_op jit(solution)/shard_map/all_to_all | solution.py:113
  106.8 44.3 %reduce-scatter.3.cloned.1.call-start = ((), (), s32[]{:S(2)}) async-start(), calls=%async_computation.5 | async-start | bytes 1310720 | tf_op jit(solution)/shard_map/reduce_scatter | solution.py:123
  122.8 3.2 %copy-start.7 = (bf16[3,768]{1,0:T(4,128)(2,1)S(1)}, bf16[3,768]{1,0:T(4,128)(2,1)}, u32[]{:S(2)}) copy-start(bf16[3,768]{1,0:T(4,128)(2,1)} %param.27) | copy-start | bytes 13828
  122.8 3.2 %copy-start.8 = (bf16[3,768]{1,0:T(4,128)(2,1)S(1)}, bf16[3,768]{1,0:T(4,128)(2,1)}, u32[]{:S(2)}) copy-start(bf16[3,768]{1,0:T(4,128)(2,1)} %param.26) | copy-start | bytes 13828
  122.8 29.5 %copy-start.6 = (f32[2048]{0:T(1024)S(1)}, f32[2048]{0:T(1024)}, u32[]{:S(2)}) copy-start(f32[2048]{0:T(1024)} %param.23) | copy-start | bytes 24580
  125.9 69.6 %reduce-scatter.5.cloned.1.call-start = ((), (), s32[]{:S(2)}) async-start(), calls=%async_computation.6 | async-start | bytes 1310720 | tf_op jit(solution)/shard_map/reduce_scatter | solution.py:151
  159.1 2.8 %copy-start.1 = (bf16[2048,768]{1,0:T(8,128)(2,1)S(1)}, bf16[2048,768]{1,0:T(8,128)(2,1)}, u32[]{:S(2)}) copy-start(bf16[2048,768]{1,0:T(8,128)(2,1)} %param.25) | copy-start | bytes 9437188
  162.5 4.7 %collective-permute-start = (bf16[2,2,768]{2,1,0:T(2,128)(2,1)S(1)}, bf16[2,2,768]{2,1,0:T(2,128)(2,1)S(1)}, u32[]{:S(2)}, u32[]{:S(2)}) collective-permute-start(bf16[2,2,768]{2,1,0:T(2,128)(2,1)S(1)} %pad_maximum_fusion.1), channel_id=1, source_target_pairs={{0,4},{4,8},{8,12},{12,16},{16,20},{20,24},{24,28},{1,5},{5,9},{9,... | collective-permute-start | bytes 18440 | tf_op jit(solution)/shard_map/ppermute | solution.py:22
  167.6 29.0 %copy-start.5 = (f32[2048]{0:T(1024)S(1)}, f32[2048]{0:T(1024)}, u32[]{:S(2)}) copy-start(f32[2048]{0:T(1024)} %param.29) | copy-start | bytes 24580
Sparse Core Ops, SparseCore 0:
  126.1 25.0 reduce-scatter.2
  169.3 26.1 reduce-scatter.4
where the time goes:
time: 206 us; the launch traced here: 205 us
  blocking collectives  80 us (39%)
  waiting for transfers between devices  67.7 us (33%)
  matrix products  18 us (9%)
  starting transfers between devices  14.3 us (7%)
  between operations  13.7 us (7%)
  other arithmetic  10.6 us (5%)
    all_gather x1, blocking collectives, shards(): lax.all_gather(value_rows, 'sp', axis=0, tiled=True)  33.2 us
    all_gather x1, blocking collectives, shards(): lax.all_gather(key_rows, 'sp', axis=0, tiled=True)  33 us
    reduce_scatter x1, waiting for transfers between devices, shards(): lax.psum_scatter(jnp.dot(row_block, down_weight, preferred_element_type=j...  26.3 us
    reduce_scatter x1, waiting for transfers between devices, shards(): lax.psum_scatter(jnp.einsum('hrd,hdc->rc', row_block, out_heads, preferre...  25.2 us
    all_to_all x1, waiting for transfers between devices, shards(): lax.all_to_all(weighted, 'tp', split_axis=1, concat_axis=0, tiled=True)  14.4 us
    all_gather x1, blocking collectives, shards(): queries = lax.all_gather(own_query, 'tp', axis=0, tiled=True)  7.17 us
    all_gather x1, blocking collectives, shards(): lax.all_gather(normalize(residual_rows, mixer_gain), 'tp', axis=0, tiled=...  6.61 us
    all_to_all x1, starting transfers between devices, shards(): lax.all_to_all(weighted, 'tp', split_axis=1, concat_axis=0, tiled=True)  4.23 us
  transfers between devices with their start and end apart: 6, of which 5 were waited for; matrix products, arithmetic and copies ran while one was open for 3% of the time, Pallas kernels for 0%

commit v1 on v0

v1 whole, which is shorter than its diff:
```python
import functools

import jax
import jax.numpy as jnp
from jax import lax
from jax.experimental import pallas as pl
from jax.experimental.pallas import tpu as pltpu
from jax.sharding import PartitionSpec as P

MESH = pl.DeviceIdType.MESH
EPS = 1e-06
HALO = 16
CORES = 2
F32 = jnp.float32
BF16 = jnp.bfloat16


def normed(values, gain):
    wide = values.astype(F32)
    scale = lax.rsqrt(jnp.mean(wide * wide, axis=-1, keepdims=True) + EPS)
    return (wide * scale * gain).astype(BF16)


def layer(
    dims,
    target_h,
    source_h,
    qgain_h,
    sgain_h,
    qw_h,
    kw_h,
    vw_h,
    ow_h,
    mgain_h,
    gw_h,
    uw_h,
    gtaps_h,
    utaps_h,
    dw_h,
    fgain_h,
    out_ref,
    tgt,
    src,
    qgain,
    sgain,
    qw,
    kw,
    vw,
    ow,
    mgain,
    gw,
    uw,
    gtaps,
    utaps,
    dw,
    fgain,
    kvh,
    kv,
    q2,
    top,
    tot,
    acc,
    att,
    part,
    half_s,
    half_r,
    chip_s,
    chip_r,
    res,
    rows_in,
    conv_g,
    conv_u,
    hid,
    tail_s,
    tail_r,
    end_s,
    end_r,
    load_sem,
    kx_s,
    kx_r,
    cw_s,
    cw_r,
    cc_s,
    cc_r,
    d2_s,
    d2_r,
    b_s,
    b_r,
    bx_s,
    bx_r,
    m_s,
    m_r,
    h_s,
    h_r,
    f_s,
    f_r,
    fx_s,
    fx_r,
):
    n, chips, kv_heads, head, heads_here, cols = dims
    tgt_rows, width = tgt.shape
    r = src.shape[0]
    rs = tgt_rows // (CORES * chips)
    half_rows = chips * rs
    chunks = width // cols
    sp = lax.axis_index("sp")
    tp = lax.axis_index("tp")
    chip = tp // CORES
    core = tp % CORES
    mate = tp + 1 - 2 * core

    def chip_at(k):
        return (chip + k) % chips

    def ring_at(p):
        if n % 2:
            return p
        upper = p // (n // 2)
        return 2 * (p * (1 - upper) + (n - 1 - p) * upper) + upper

    if n % 2:
        pos = sp
    else:
        pos = (sp // 2) * (1 - sp % 2) + (n - 1 - sp // 2) * (sp % 2)
    ahead = ring_at((pos + 1) % n)
    behind = ring_at((pos + n - 1) % n)

    def load(index, hbm, vmem):
        copy = pltpu.make_async_copy(hbm, vmem, load_sem.at[index])
        copy.start()
        return copy

    first = [
        load(i, a, b)
        for i, (a, b) in enumerate(((source_h, src), (sgain_h, sgain), (kw_h, kw), (vw_h, vw)))
    ]
    second = [
        load(4 + i, a, b)
        for i, (a, b) in enumerate(((target_h, tgt), (qgain_h, qgain), (qw_h, qw)))
    ]

    barrier = pltpu.get_barrier_semaphore()
    following, previous = (sp + 1) % n, (sp + n - 1) % n
    peers = [(ahead, tp), (behind, tp), (sp, mate)]
    peers += [(sp, chip_at(k) * CORES + core) for k in range(1, chips)]
    peers += [(s, t) for s in (following, previous) for t in (tp, mate)]
    for peer in peers:
        pl.semaphore_signal(barrier, inc=1, device_id=peer, device_id_type=MESH)

    def remote(source_ref, dest_ref, send, recv, device):
        return pltpu.make_async_remote_copy(
            src_ref=source_ref,
            dst_ref=dest_ref,
            send_sem=send,
            recv_sem=recv,
            device_id=device,
            device_id_type=MESH,
        )

    def block(slot, lineage, j):
        start = ((slot * CORES + lineage) * chips + j) * r
        if not isinstance(start, int):
            start = pl.multiple_of(start, r)
        return kv.at[pl.ds(start, r), :]

    def head_of(c):
        return (c * CORES * kv_heads) // (chips * CORES)

    def chip_copy(k):
        there = chip_at(k)
        return remote(
            kvh.at[head_of(there)],
            block(0, 0, k),
            kx_s.at[k],
            kx_r.at[k],
            (sp, there * CORES + core),
        )

    last = n // 2 if n % 2 == 0 else 0
    full = (n - 1) // 2
    last_cw = (chips + 1) // 2

    def cw_slot(d):
        return 2 * d - 1

    def cc_slot(d):
        return n - 1 if isinstance(d, int) and d == last else 2 * d

    def cw_copy(d, j):
        held = 0 if isinstance(d, int) and d == 1 else cw_slot(d - 1)
        return remote(
            block(held, 0, j), block(cw_slot(d), 0, j), cw_s.at[d, j], cw_r.at[d, j], (ahead, tp)
        )

    def cc_copy(d, j):
        held = 0 if isinstance(d, int) and d == 1 else 2 * (d - 1)
        return remote(
            block(held, 0, j), block(cc_slot(d), 0, j), cc_s.at[d, j], cc_r.at[d, j], (behind, tp)
        )

    def mate_copy(slot, j):
        return remote(
            block(slot, 0, j), block(slot, 1, j), d2_s.at[slot, j], d2_r.at[slot, j], (sp, mate)
        )

    for copy in first:
        copy.wait()
    rest = [
        load(7 + i, a, b)
        for i, (a, b) in enumerate(
            (
                (ow_h, ow),
                (mgain_h, mgain),
                (gw_h, gw),
                (uw_h, uw),
                (gtaps_h, gtaps),
                (utaps_h, utaps),
                (dw_h, dw),
                (fgain_h, fgain),
            )
        )
    ]
    source_in = normed(src[...], sgain[...])
    keys = jnp.dot(source_in, kw[...], preferred_element_type=F32).astype(BF16)
    values = jnp.dot(source_in, vw[...], preferred_element_type=F32).astype(BF16)
    for g in range(kv_heads):
        kvh[g, :, :head] = keys[:, g * head : (g + 1) * head]
        kvh[g, :, head:] = values[:, g * head : (g + 1) * head]
    kv[0:r, :] = kvh[head_of(chip)]
    pl.semaphore_wait(barrier, len(peers))

    def launch(j):
        if n > 2 or j < last_cw:
            cw_copy(1, j).start()
        if n > 2 or j >= last_cw:
            cc_copy(1, j).start()
        mate_copy(0, j).start()

    for k in range(1, chips):
        chip_copy(k).start()
    launch(0)

    for copy in second:
        copy.wait()
    queries = jnp.dot(normed(tgt[...], qgain[...]), qw[...], preferred_element_type=F32).astype(
        BF16
    )
    for h in range(heads_here):
        q2[h * tgt_rows : (h + 1) * tgt_rows, :] = queries[:, h * head : (h + 1) * head]
    top[...] = jnp.full(top.shape, -1e30, F32)
    tot[...] = jnp.zeros(tot.shape, F32)
    acc[...] = jnp.zeros(acc.shape, F32)

    for k in range(1, chips):
        chip_copy(k).wait_recv()
        launch(k)

    slot_rows = CORES * chips * r

    def attend(slot, slots):
        start = slot * slot_rows
        if not isinstance(start, int):
            start = pl.multiple_of(start, slot_rows)
        for s in range(slots):
            for j in range(chips):
                mate_copy(slot + s, j).wait_recv()
        here = pl.ds(start, slots * slot_rows)
        scores = lax.dot_general(
            q2[...], kv[here, :head], (((1,), (1,)), ((), ())), preferred_element_type=F32
        ) * (head**-0.5)
        old = top[...]
        new = jnp.maximum(old, jnp.max(scores, axis=-1, keepdims=True))
        shrink = jnp.exp(old - new)
        probs = jnp.exp(scores - new)
        top[...] = new
        tot[...] = tot[...] * shrink + jnp.sum(probs, axis=-1, keepdims=True)
        acc[...] = acc[...] * shrink + jnp.dot(
            probs.astype(BF16), kv[here, head:], preferred_element_type=F32
        )

    def step(d, cw_on, cc_on):
        for j in range(chips):
            cw_copy(d, j).wait_recv()
            if j in cw_on:
                cw_copy(d + 1, j).start()
            mate_copy(cw_slot(d), j).start()
            cc_copy(d, j).wait_recv()
            if j in cc_on:
                cc_copy(d + 1, j).start()
            mate_copy(cc_slot(d), j).start()

    every = range(chips)
    few = range(0, last_cw) if last else range(0)
    others = range(last_cw, chips) if last else range(0)
    if full >= 1:
        step(1, every if full > 1 else few, every if full > 1 else others)
        attend(0, 1)
        if full > 6:

            def middle(d, carry):
                step(d, every, every)
                attend(2 * d - 3, 2)
                return carry

            lax.fori_loop(2, full, middle, 0)
        else:
            for d in range(2, full):
                step(d, every, every)
                attend(2 * d - 3, 2)
        if full > 1:
            step(full, few, others)
            attend(2 * full - 3, 2)
        tail_slot, tail_count = 2 * full - 1, 2
    else:
        tail_slot, tail_count = 0, 1
    if last:
        for j in every:
            (cw_copy if j < last_cw else cc_copy)(last, j).wait_recv()
            mate_copy(n - 1, j).start()
    attend(tail_slot, tail_count)
    if last:
        attend(n - 1, 1)

    attended = (acc[...] / tot[...]).astype(BF16)
    for h in range(heads_here):
        att[:, h * head : (h + 1) * head] = attended[h * tgt_rows : (h + 1) * tgt_rows, :]
    for copy in rest:
        copy.wait()

    def piece(c, side):
        return pl.ds(pl.multiple_of((c * CORES + side) * rs, rs), rs)

    def multiply_out(lhs, weight, send, recv, send_sem, recv_sem):
        for c in range(chunks):
            here = slice(c * cols, (c + 1) * cols)
            part[c] = jnp.dot(lhs, weight[:, here], preferred_element_type=F32)
            for k in range(chips):
                send[c, k * rs : (k + 1) * rs, :] = part[c, piece(k, 1 - core), :].astype(BF16)
            remote(send.at[c], recv.at[c], send_sem.at[c], recv_sem.at[c], (sp, mate)).start()

    def mate_wait(c, send, recv, send_sem, recv_sem):
        remote(send.at[c], recv.at[c], send_sem.at[c], recv_sem.at[c], (sp, mate)).wait_recv()

    multiply_out(att[...], ow, half_s, half_r, b_s, b_r)

    def wide_copy(k, c):
        return remote(
            chip_s.at[c],
            chip_r.at[k - 1, c],
            bx_s.at[k, c],
            bx_r.at[k, c],
            (sp, chip_at(k) * CORES + core),
        )

    for c in range(chunks):
        mate_wait(c, half_s, half_r, b_s, b_r)
        for k in range(chips):
            at = slice(k * rs, (k + 1) * rs)
            both = part[c, piece(k, core), :] + half_r[c, at, :].astype(F32)
            res[at, c * cols : (c + 1) * cols] = both
            chip_s[c, at, :] = both.astype(BF16)
        for k in range(1, chips):
            wide_copy(k, c).start()
    squares = jnp.zeros((half_rows, 1), F32)
    for c in range(chunks):
        here = slice(c * cols, (c + 1) * cols)
        projected = res[:, here]
        for k in range(1, chips):
            wide_copy(k, c).wait_recv()
            projected = projected + chip_r[k - 1, c].astype(F32)
        mine = jnp.concatenate([tgt[piece(k, core), here] for k in range(chips)], axis=0)
        residual = (mine.astype(F32) + projected).astype(BF16).astype(F32)
        res[:, here] = residual
        squares = squares + jnp.sum(residual * residual, axis=-1, keepdims=True)
    scale = lax.rsqrt(squares / width + EPS)

    def spot(k):
        return pl.ds(pl.multiple_of(HALO + (k * CORES + core) * rs, HALO), rs)

    def row_copy(k):
        return remote(
            rows_in.at[spot(k), :], rows_in.at[spot(k), :], m_s.at[k], m_r.at[k], (sp, mate)
        )

    def mate_row_copy(k):
        at = pl.ds(pl.multiple_of(HALO + (k * CORES + 1 - core) * rs, HALO), rs)
        return remote(rows_in.at[at, :], rows_in.at[at, :], m_s.at[k], m_r.at[k], (sp, mate))

    def halo_copy(i, t):
        return remote(
            rows_in.at[tgt_rows : tgt_rows + HALO, :],
            rows_in.at[0:HALO, :],
            h_s.at[i],
            h_r,
            (following, t),
        )

    sends_halo = jnp.logical_and(core == 1, sp < n - 1)
    for k in reversed(range(chips)):
        at = slice(k * rs, (k + 1) * rs)
        rows_in[spot(k), :] = (res[at, :] * scale[at, :] * mgain[...]).astype(BF16)
        if k == chips - 1:

            @pl.when(sends_halo)
            def _():
                halo_copy(0, mate).start()
                halo_copy(1, tp).start()

        row_copy(k).start()

    @pl.when(sp == 0)
    def _():
        rows_in[0:HALO, :] = jnp.zeros((HALO, width), BF16)

    for k in range(chips):
        mate_row_copy(k).wait_recv()

    @pl.when(sp > 0)
    def _():
        halo_copy(0, tp).wait_recv()

    hidden_cols = hid.shape[1]
    wide = conv_g.shape[1]
    taps = gtaps.shape[0]
    for f in range(hidden_cols // wide):
        here = slice(f * wide, (f + 1) * wide)
        all_rows = rows_in[...]
        conv_g[...] = jnp.dot(all_rows, gw[:, here], preferred_element_type=F32).astype(
            BF16
        ).astype(F32)
        conv_u[...] = jnp.dot(all_rows, uw[:, here], preferred_element_type=F32).astype(
            BF16
        ).astype(F32)
        gate = jnp.zeros((tgt_rows, wide), F32)
        up = jnp.zeros((tgt_rows, wide), F32)
        for t in range(taps):
            begin = HALO - (taps - 1) + t
            gate = gate + gtaps[t : t + 1, here].astype(F32) * conv_g[begin : begin + tgt_rows, :]
            up = up + utaps[t : t + 1, here].astype(F32) * conv_u[begin : begin + tgt_rows, :]
        hid[:, here] = (gate / (1.0 + jnp.exp(-gate)) * up).astype(BF16)

    multiply_out(hid[...], dw, tail_s, tail_r, f_s, f_r)

    def end_copy(k, c):
        there = chip_at(k)
        at = pl.ds(pl.multiple_of(there * rs, rs), rs)
        return remote(
            end_s.at[c, at, :],
            end_r.at[k - 1, c],
            fx_s.at[k, c],
            fx_r.at[k, c],
            (sp, there * CORES + core),
        )

    for c in range(chunks):
        mate_wait(c, tail_s, tail_r, f_s, f_r)
        for k in range(chips):
            at = slice(k * rs, (k + 1) * rs)
            both = part[c, piece(k, core), :] + tail_r[c, at, :].astype(F32)
            part[c, piece(k, core), :] = both
            end_s[c, at, :] = both.astype(BF16)
        for k in range(1, chips):
            end_copy(k, c).start()
    own = pl.ds(pl.multiple_of(chip * rs, rs), rs)
    squares = jnp.zeros((rs, 1), F32)
    sums = []
    for c in range(chunks):
        here = slice(c * cols, (c + 1) * cols)
        total = res[own, here] + part[c, piece(chip, core), :]
        for k in range(1, chips):
            end_copy(k, c).wait_recv()
            total = total + end_r[k - 1, c].astype(F32)
        squares = squares + jnp.sum(total * total, axis=-1, keepdims=True)
        sums.append(total)
    scale = lax.rsqrt(squares / width + EPS)
    for c in range(chunks):
        here = slice(c * cols, (c + 1) * cols)
        out_ref[:, here] = (sums[c] * scale * fgain[:, here]).astype(BF16)

    for k in range(1, chips):
        chip_copy(k).wait_send()
        for c in range(chunks):
            wide_copy(k, c).wait_send()
            end_copy(k, c).wait_send()
    for c in range(chunks):
        remote(half_s.at[c], half_r.at[c], b_s.at[c], b_r.at[c], (sp, mate)).wait_send()
        remote(tail_s.at[c], tail_r.at[c], f_s.at[c], f_r.at[c], (sp, mate)).wait_send()
    for k in range(chips):
        row_copy(k).wait_send()

    @pl.when(sends_halo)
    def _():
        halo_copy(0, mate).wait_send()
        halo_copy(1, tp).wait_send()

    def drain(d, carry):
        for j in every:
            cw_copy(d, j).wait_send()
            cc_copy(d, j).wait_send()
        return carry

    def drain_mate(slot, carry):
        for j in every:
            mate_copy(slot, j).wait_send()
        return carry

    if full >= 1:
        drain(1, 0)
    if full >= 2:
        lax.fori_loop(2, full + 1, drain, 0)
    if last:
        for j in every:
            (cw_copy if j < last_cw else cc_copy)(last, j).wait_send()
    lax.fori_loop(0, n, drain_mate, 0)


def solution(mesh):
    n = mesh.shape["sp"]
    chips = mesh.shape["tp"] // CORES
    head = 256

    def shards(*args):
        args = [a[None, :] if a.ndim == 1 else a for a in args]
        (target, source, _, _, qw, kw, _, ow, _, gw, _, _, _, dw, _) = args
        tgt_rows, width = target.shape
        r = source.shape[0]
        kv_heads = kw.shape[1] // head
        heads_here = qw.shape[1] // head
        rs = tgt_rows // (CORES * chips)
        half = chips * rs
        cols = 512
        chunks = width // cols
        ff = gw.shape[1]
        wide = 256 if ff % 256 == 0 else 128
        q_rows = heads_here * tgt_rows
        dists = n // 2 + 1
        dma = pltpu.SemaphoreType.DMA
        scratch = [pltpu.VMEM(a.shape, a.dtype) for a in args]
        scratch += [
            pltpu.VMEM((kv_heads, r, 2 * head), BF16),
            pltpu.VMEM((n * CORES * chips * r, 2 * head), BF16),
            pltpu.VMEM((q_rows, head), BF16),
            pltpu.VMEM((q_rows, 1), F32),
            pltpu.VMEM((q_rows, 1), F32),
            pltpu.VMEM((q_rows, head), F32),
            pltpu.VMEM((tgt_rows, heads_here * head), BF16),
            pltpu.VMEM((chunks, tgt_rows, cols), F32),
            pltpu.VMEM((chunks, half, cols), BF16),
            pltpu.VMEM((chunks, half, cols), BF16),
            pltpu.VMEM((chunks, half, cols), BF16),
            pltpu.VMEM((max(chips - 1, 1), chunks, half, cols), BF16),
            pltpu.VMEM((half, width), F32),
            pltpu.VMEM((HALO + tgt_rows, width), BF16),
            pltpu.VMEM((HALO + tgt_rows, wide), F32),
            pltpu.VMEM((HALO + tgt_rows, wide), F32),
            pltpu.VMEM((tgt_rows, ff), BF16),
            pltpu.VMEM((chunks, half, cols), BF16),
            pltpu.VMEM((chunks, half, cols), BF16),
            pltpu.VMEM((chunks, half, cols), BF16),
            pltpu.VMEM((max(chips - 1, 1), chunks, rs, cols), BF16),
            dma((len(args),)),
            dma((chips,)),
            dma((chips,)),
        ]
        scratch += [dma((dists, chips))] * 4
        scratch += [dma((n, chips))] * 2
        scratch += [dma((chunks,))] * 2
        scratch += [dma((chips, chunks))] * 2
        scratch += [dma((chips,))] * 2
        scratch += [dma((2,)), dma]
        scratch += [dma((chunks,))] * 2
        scratch += [dma((chips, chunks))] * 2
        return pl.pallas_call(
            functools.partial(layer, (n, chips, kv_heads, head, heads_here, cols)),
            out_shape=jax.ShapeDtypeStruct((rs, width), BF16),
            in_specs=[pl.BlockSpec(memory_space=pl.ANY)] * len(args),
            out_specs=pl.BlockSpec(memory_space=pltpu.VMEM),
            scratch_shapes=scratch,
            compiler_params=pltpu.CompilerParams(
                collective_id=0, has_side_effects=True, vmem_limit_bytes=60 * 1024 * 1024
            ),
        )(*args)

    in_specs = (
        P("sp", None),
        P(("sp", "tp"), None),
        P(),
        P(),
        P(None, "tp"),
        P(),
        P(),
        P("tp", None),
        P(),
        P(None, "tp"),
        P(None, "tp"),
        P(None, "tp"),
        P(None, "tp"),
        P("tp", None),
        P(),
    )
    return jax.shard_map(
        shards, mesh=mesh, in_specs=in_specs, out_specs=P(("sp", "tp"), None), check_vma=False
    )
```

time: 206 us -> 47.8 us (0.23)
  blocking collectives: 80 us -> 0 us
  waiting for transfers between devices: 67.7 us -> 0 us
  Pallas kernels: 0 us -> 46.1 us
  matrix products: 18 us -> 0 us
  starting transfers between devices: 14.3 us -> 0 us
  between operations: 13.7 us -> 0.01 us
  other arithmetic: 10.6 us -> 0 us
    all_gather x4 -> x0, blocking collectives: 80 us -> none  [the longest x1 33.2 us: shards(): lax.all_gather(value_rows, 'sp', axis=0, tiled=True)]
    reduce_scatter x2 -> x0, waiting for transfers between devices: 51.4 us -> none  [the longest x1 26.3 us: shards(): lax.psum_scatter(jnp.dot(row_block, down_weight, preferred_element_type=j...]
    pallas_call x0 -> x1, Pallas kernels: none -> 46.1 us  [shards(): pl.pallas_call(functools.partial(layer, (n, chips, kv_heads, head, heads_...]
    dot_general x9 -> x0, matrix products: 18 us -> none  [the longest x1 3.32 us: absorb(): jnp.einsum('gqn,ngd->gqd', probabilities.astype(jnp.bfloat16), value_head...]
    all_to_all x3 -> x0, waiting for transfers between devices: 14.9 us -> none  [the longest x1 14.4 us: shards(): lax.all_to_all(weighted, 'tp', split_axis=1, concat_axis=0, tiled=True)]
    all_to_all x3 -> x0, starting transfers between devices: 10.9 us -> none  [the longest x1 4.23 us: shards(): lax.all_to_all(weighted, 'tp', split_axis=1, concat_axis=0, tiled=True)]
    reduce_sum x7 -> x0, other arithmetic: 7.07 us -> none  [the longest x4 3.66 us: normalize(): jnp.mean(widened * widened, axis=-1, keepdims=True) + EPS]
    ppermute x1 -> x0, starting transfers between devices: 3.37 us -> none  [passed_along(): return lax.ppermute(shard, axis, pairs)]
  transfers between devices with their start and end apart: 6 -> 0, of which waited for: 5 -> 0; matrix products, arithmetic and copies ran while one was open for 3% -> 0% of each run, Pallas kernels for 0% -> 0%
where the time goes in v1:
time: 47.8 us; the launch traced here: 47.7 us
  Pallas kernels  46.1 us (96%)
  local copies, waits for them, and re-layouts  1.57 us (3%)
    pallas_call x1, Pallas kernels, shards(): pl.pallas_call(functools.partial(layer, (n, chips, kv_heads, head, heads_...  46.1 us
    unnamed x1, local copies, waits for them, and re-layouts  1.57 us

profile of v1, /device:TPU:0, one launch (start us, length us, event | category | flops | bytes accessed | tf_op | source)
XLA Modules:
  0.0 47.7 jit_solution(14706190528867976414)
XLA Ops:
  0.0 46.1 %shard_map.145 = bf16[32,2048]{1,0:T(8,128)(2,1)} custom-call(bf16[128,2048]{1,0:T(8,128)(2,1)} %target_h.1, bf16[64,2048]{1,0:T(8,128)(2,1)} %source_h.1, f32[1,2048]{1,0:T(1,128)} %bitcast.4, f32[1,2048]{1,0:T(1,128)} %bitcast.5, bf16[2048,512]{1,0:T(8,128)(2,1)} %qw_h.1, bf16[2048,512]{1,0:T(8,128)(2,1)} %kw_h.1, bf16[2048,512]{1,0:T(8,128)(2,1)} %vw_h.1, ...), custom_call_target="tpu_custom_call" | custom-call | tf_op jit(solution)/shard_map/pallas_call | solution.py:573
  46.1 1.6 %copy.17 = bf16[32,2048]{1,0:T(8,128)(2,1)} copy(bf16[32,2048]{1,0:T(8,128)(2,1)} %shard_map.145) | data formatting | bytes 262144

commit v2 on v1

--- a/solution.py
+++ b/solution.py
@@ -10,6 +10,7 @@
 MESH = pl.DeviceIdType.MESH
 EPS = 1e-06
 HALO = 16
+RUN = 16
 CORES = 2
 F32 = jnp.float32
 BF16 = jnp.bfloat16
@@ -97,11 +98,13 @@
     fx_s,
     fx_r,
 ):
-    n, chips, kv_heads, head, heads_here, cols = dims
+    n, chips, kv_heads, head, heads_here, cols, sub = dims
     tgt_rows, width = tgt.shape
     r = src.shape[0]
     rs = tgt_rows // (CORES * chips)
     half_rows = chips * rs
+    run = r // sub
+    runs = chips * sub
     chunks = width // cols
     sp = lax.axis_index("sp")
     tp = lax.axis_index("tp")
@@ -130,20 +133,29 @@
         copy.start()
         return copy
 
-    first = [
-        load(i, a, b)
-        for i, (a, b) in enumerate(((source_h, src), (sgain_h, sgain), (kw_h, kw), (vw_h, vw)))
+    def head_of(c):
+        return (c * CORES * kv_heads) // (chips * CORES)
+
+    own_head = head_of(chip)
+    order = [(own_head + 1 + g) % kv_heads for g in range(kv_heads)]
+
+    def columns(g):
+        return pl.ds(pl.multiple_of(g * head, head), head)
+
+    first = [load(0, source_h, src), load(1, sgain_h, sgain)]
+    by_head = [
+        [
+            load(2 + 2 * i, kw_h.at[:, columns(g)], kw.at[:, columns(g)]),
+            load(3 + 2 * i, vw_h.at[:, columns(g)], vw.at[:, columns(g)]),
+        ]
+        for i, g in enumerate(order)
     ]
-    second = [
-        load(4 + i, a, b)
-        for i, (a, b) in enumerate(((target_h, tgt), (qgain_h, qgain), (qw_h, qw)))
-    ]
+    used = 2 + 2 * kv_heads
 
     barrier = pltpu.get_barrier_semaphore()
-    following, previous = (sp + 1) % n, (sp + n - 1) % n
+    following = (sp + 1) % n
     peers = [(ahead, tp), (behind, tp), (sp, mate)]
     peers += [(sp, chip_at(k) * CORES + core) for k in range(1, chips)]
-    peers += [(s, t) for s in (following, previous) for t in (tp, mate)]
     for peer in peers:
         pl.semaphore_signal(barrier, inc=1, device_id=peer, device_id_type=MESH)
 
@@ -158,27 +170,28 @@
         )
 
     def block(slot, lineage, j):
-        start = ((slot * CORES + lineage) * chips + j) * r
+        start = ((slot * CORES + lineage) * runs + j) * run
         if not isinstance(start, int):
-            start = pl.multiple_of(start, r)
-        return kv.at[pl.ds(start, r), :]
-
-    def head_of(c):
-        return (c * CORES * kv_heads) // (chips * CORES)
-
-    def chip_copy(k):
-        there = chip_at(k)
-        return remote(
-            kvh.at[head_of(there)],
-            block(0, 0, k),
-            kx_s.at[k],
-            kx_r.at[k],
+            start = pl.multiple_of(start, run)
+        return kv.at[pl.ds(start, run), :]
+
+    def chip_copy(j):
+        there = chip_at(j // sub)
+        return remote(
+            kvh.at[head_of(there), (j % sub) * run : (j % sub + 1) * run, :],
+            block(0, 0, j),
+            kx_s.at[j],
+            kx_r.at[j],
             (sp, there * CORES + core),
         )
 
     last = n // 2 if n % 2 == 0 else 0
     full = (n - 1) // 2
-    last_cw = (chips + 1) // 2
+    if sub > 1:
+        half_cw = [j for j in range(runs) if j % sub < sub // 2]
+    else:
+        half_cw = list(range((runs + 1) // 2))
+    half_cc = [j for j in range(runs) if j not in half_cw]
 
     def cw_slot(d):
         return 2 * d - 1
@@ -203,10 +216,37 @@
             block(slot, 0, j), block(slot, 1, j), d2_s.at[slot, j], d2_r.at[slot, j], (sp, mate)
         )
 
+    def launch(j):
+        if n > 2 or j in half_cw:
+            cw_copy(1, j).start()
+        if n > 2 or j in half_cc:
+            cc_copy(1, j).start()
+        mate_copy(0, j).start()
+
     for copy in first:
         copy.wait()
+    source_in = normed(src[...], sgain[...])
+    second = [
+        load(used + i, a, b)
+        for i, (a, b) in enumerate(((target_h, tgt), (qgain_h, qgain), (qw_h, qw)))
+    ]
+    early = chips == kv_heads
+    for i, g in enumerate(order):
+        for copy in by_head[i]:
+            copy.wait()
+        keys = jnp.dot(source_in, kw[:, columns(g)], preferred_element_type=F32)
+        kvh[g, :, :head] = keys.astype(BF16)
+        values = jnp.dot(source_in, vw[:, columns(g)], preferred_element_type=F32)
+        kvh[g, :, head:] = values.astype(BF16)
+        if i == (kv_heads - 2 if early else kv_heads - 1):
+            pl.semaphore_wait(barrier, len(peers))
+            for j in range(sub, runs):
+                chip_copy(j).start()
+    kv[0:r, :] = kvh[own_head]
+    for j in range(sub):
+        launch(j)
     rest = [
-        load(7 + i, a, b)
+        load(used + 3 + i, a, b)
         for i, (a, b) in enumerate(
             (
                 (ow_h, ow),
@@ -220,25 +260,6 @@
             )
         )
     ]
-    source_in = normed(src[...], sgain[...])
-    keys = jnp.dot(source_in, kw[...], preferred_element_type=F32).astype(BF16)
-    values = jnp.dot(source_in, vw[...], preferred_element_type=F32).astype(BF16)
-    for g in range(kv_heads):
-        kvh[g, :, :head] = keys[:, g * head : (g + 1) * head]
-        kvh[g, :, head:] = values[:, g * head : (g + 1) * head]
-    kv[0:r, :] = kvh[head_of(chip)]
-    pl.semaphore_wait(barrier, len(peers))
-
-    def launch(j):
-        if n > 2 or j < last_cw:
-            cw_copy(1, j).start()
-        if n > 2 or j >= last_cw:
-            cc_copy(1, j).start()
-        mate_copy(0, j).start()
-
-    for k in range(1, chips):
-        chip_copy(k).start()
-    launch(0)
 
     for copy in second:
         copy.wait()
@@ -251,9 +272,9 @@
     tot[...] = jnp.zeros(tot.shape, F32)
     acc[...] = jnp.zeros(acc.shape, F32)
 
-    for k in range(1, chips):
-        chip_copy(k).wait_recv()
-        launch(k)
+    for j in range(sub, runs):
+        chip_copy(j).wait_recv()
+        launch(j)
 
     slot_rows = CORES * chips * r
 
@@ -262,7 +283,7 @@
         if not isinstance(start, int):
             start = pl.multiple_of(start, slot_rows)
         for s in range(slots):
-            for j in range(chips):
+            for j in range(runs):
                 mate_copy(slot + s, j).wait_recv()
         here = pl.ds(start, slots * slot_rows)
         scores = lax.dot_general(
@@ -279,7 +300,7 @@
         )
 
     def step(d, cw_on, cc_on):
-        for j in range(chips):
+        for j in range(runs):
             cw_copy(d, j).wait_recv()
             if j in cw_on:
                 cw_copy(d + 1, j).start()
@@ -289,9 +310,9 @@
                 cc_copy(d + 1, j).start()
             mate_copy(cc_slot(d), j).start()
 
-    every = range(chips)
-    few = range(0, last_cw) if last else range(0)
-    others = range(last_cw, chips) if last else range(0)
+    every = range(runs)
+    few = half_cw if last else []
+    others = half_cc if last else []
     if full >= 1:
         step(1, every if full > 1 else few, every if full > 1 else others)
         attend(0, 1)
@@ -315,7 +336,7 @@
         tail_slot, tail_count = 0, 1
     if last:
         for j in every:
-            (cw_copy if j < last_cw else cc_copy)(last, j).wait_recv()
+            (cw_copy if j in half_cw else cc_copy)(last, j).wait_recv()
             mate_copy(n - 1, j).start()
     attend(tail_slot, tail_count)
     if last:
@@ -477,8 +498,9 @@
         here = slice(c * cols, (c + 1) * cols)
         out_ref[:, here] = (sums[c] * scale * fgain[:, here]).astype(BF16)
 
+    for j in range(sub, runs):
+        chip_copy(j).wait_send()
     for k in range(1, chips):
-        chip_copy(k).wait_send()
         for c in range(chunks):
             wide_copy(k, c).wait_send()
             end_copy(k, c).wait_send()
@@ -510,7 +532,7 @@
         lax.fori_loop(2, full + 1, drain, 0)
     if last:
         for j in every:
-            (cw_copy if j < last_cw else cc_copy)(last, j).wait_send()
+            (cw_copy if j in half_cw else cc_copy)(last, j).wait_send()
     lax.fori_loop(0, n, drain_mate, 0)
 
 
@@ -534,6 +556,8 @@
         wide = 256 if ff % 256 == 0 else 128
         q_rows = heads_here * tgt_rows
         dists = n // 2 + 1
+        sub = max(r // RUN, 1)
+        runs = chips * sub
         dma = pltpu.SemaphoreType.DMA
         scratch = [pltpu.VMEM(a.shape, a.dtype) for a in args]
         scratch += [
@@ -558,12 +582,12 @@
             pltpu.VMEM((chunks, half, cols), BF16),
             pltpu.VMEM((chunks, half, cols), BF16),
             pltpu.VMEM((max(chips - 1, 1), chunks, rs, cols), BF16),
-            dma((len(args),)),
-            dma((chips,)),
-            dma((chips,)),
+            dma((len(args) + 2 * kv_heads,)),
+            dma((runs,)),
+            dma((runs,)),
         ]
-        scratch += [dma((dists, chips))] * 4
-        scratch += [dma((n, chips))] * 2
+        scratch += [dma((dists, runs))] * 4
+        scratch += [dma((n, runs))] * 2
         scratch += [dma((chunks,))] * 2
         scratch += [dma((chips, chunks))] * 2
         scratch += [dma((chips,))] * 2
@@ -571,7 +595,7 @@
         scratch += [dma((chunks,))] * 2
         scratch += [dma((chips, chunks))] * 2
         return pl.pallas_call(
-            functools.partial(layer, (n, chips, kv_heads, head, heads_here, cols)),
+            functools.partial(layer, (n, chips, kv_heads, head, heads_here, cols, sub)),
             out_shape=jax.ShapeDtypeStruct((rs, width), BF16),
             in_specs=[pl.BlockSpec(memory_space=pl.ANY)] * len(args),
             out_specs=pl.BlockSpec(memory_space=pltpu.VMEM),

time: 47.8 us -> 46.2 us (0.967)
  Pallas kernels: 46.1 us -> 44.5 us
    pallas_call x1, Pallas kernels: 46.1 us -> 44.5 us  [shards(): pl.pallas_call(functools.partial(layer, (n, chips, kv_heads, head, heads_...]
where the time goes in v2:
time: 46.2 us; the launch traced here: 46.1 us
  Pallas kernels  44.5 us (96%)
  local copies, waits for them, and re-layouts  1.57 us (3%)
    pallas_call x1, Pallas kernels, shards(): pl.pallas_call(functools.partial(layer, (n, chips, kv_heads, head, heads_...  44.5 us
    unnamed x1, local copies, waits for them, and re-layouts  1.57 us

profile of v2, /device:TPU:0, one launch (start us, length us, event | category | flops | bytes accessed | tf_op | source)
XLA Modules:
  0.0 46.1 jit_solution(1917345577798000466)
XLA Ops:
  0.0 44.5 %shard_map.145 = bf16[32,2048]{1,0:T(8,128)(2,1)} custom-call(bf16[128,2048]{1,0:T(8,128)(2,1)} %target_h.1, bf16[64,2048]{1,0:T(8,128)(2,1)} %source_h.1, f32[1,2048]{1,0:T(1,128)} %bitcast.4, f32[1,2048]{1,0:T(1,128)} %bitcast.5, bf16[2048,512]{1,0:T(8,128)(2,1)} %qw_h.1, bf16[2048,512]{1,0:T(8,128)(2,1)} %kw_h.1, bf16[2048,512]{1,0:T(8,128)(2,1)} %vw_h.1, ...), custom_call_target="tpu_custom_call" | custom-call | tf_op jit(solution)/shard_map/pallas_call | solution.py:597
  44.5 1.6 %copy.17 = bf16[32,2048]{1,0:T(8,128)(2,1)} copy(bf16[32,2048]{1,0:T(8,128)(2,1)} %shard_map.145) | data formatting | bytes 262144

commit v3 on v2

--- a/solution.py
+++ b/solution.py
@@ -10,7 +10,7 @@
 MESH = pl.DeviceIdType.MESH
 EPS = 1e-06
 HALO = 16
-RUN = 16
+RUN = 32
 CORES = 2
 F32 = jnp.float32
 BF16 = jnp.bfloat16
@@ -550,7 +550,7 @@
         heads_here = qw.shape[1] // head
         rs = tgt_rows // (CORES * chips)
         half = chips * rs
-        cols = 512
+        cols = width // 2
         chunks = width // cols
         ff = gw.shape[1]
         wide = 256 if ff % 256 == 0 else 128
@@ -596,7 +596,7 @@
         scratch += [dma((chips, chunks))] * 2
         return pl.pallas_call(
             functools.partial(layer, (n, chips, kv_heads, head, heads_here, cols, sub)),
-            out_shape=jax.ShapeDtypeStruct((rs, width), BF16),
+            out_shape=pltpu.VMEM((rs, width), BF16),
             in_specs=[pl.BlockSpec(memory_space=pl.ANY)] * len(args),
             out_specs=pl.BlockSpec(memory_space=pltpu.VMEM),
             scratch_shapes=scratch,

time: 46.2 us -> 43.6 us (0.944)
  Pallas kernels: 44.5 us -> 42.8 us
  local copies, waits for them, and re-layouts: 1.57 us -> 0.66 us
    pallas_call x1, Pallas kernels: 44.5 us -> 42.8 us  [shards(): pl.pallas_call(functools.partial(layer, (n, chips, kv_heads, head, heads_...]
    unnamed x1, local copies, waits for them, and re-layouts: 1.57 us -> 0.66 us
where the time goes in v3:
time: 43.6 us; the launch traced here: 43.5 us
  Pallas kernels  42.8 us (98%)
  local copies, waits for them, and re-layouts  0.66 us (2%)
    pallas_call x1, Pallas kernels, shards(): pl.pallas_call(functools.partial(layer, (n, chips, kv_heads, head, heads_...  42.8 us

profile of v3, /device:TPU:0, one launch (start us, length us, event | category | flops | bytes accessed | tf_op | source)
XLA Modules:
  0.0 43.5 jit_solution(9748488057537774224)
XLA Ops:
  0.0 42.8 %shard_map.145 = bf16[32,2048]{1,0:T(8,128)(2,1)S(1)} custom-call(bf16[128,2048]{1,0:T(8,128)(2,1)} %target_h.1, bf16[64,2048]{1,0:T(8,128)(2,1)} %source_h.1, f32[1,2048]{1,0:T(1,128)} %bitcast.4, f32[1,2048]{1,0:T(1,128)} %bitcast.5, bf16[2048,512]{1,0:T(8,128)(2,1)} %qw_h.1, bf16[2048,512]{1,0:T(8,128)(2,1)} %kw_h.1, bf16[2048,512]{1,0:T(8,128)(2,1)} %vw_h.1, ...), custom_call_target="tpu_custom_call" | custom-call | tf_op jit(solution)/shard_map/pallas_call | solution.py:597
  42.8 0.7 %copy.17 = bf16[32,2048]{1,0:T(8,128)(2,1)} copy(bf16[32,2048]{1,0:T(8,128)(2,1)S(1)} %shard_map.145) | data formatting | bytes 262144
